TPU v7x, 32 devices: a whole 2x2x4 slice. The times are simulated.
32 devices in a mesh: grp: 2 (over y), sp: 4 (over z), tp: 4 (over x, core).
Axes of the slice: x: 2, y: 2, z: 4, core: 2. Of those that a mesh axis runs over, the one named last changes fastest.
Arguments:
- tokens: bfloat16 [8, 1024, 4096], P(('grp', 'tp'), 'sp'), parts along dimension 0, may hold values from -8 to 8, as said below
- offsets: int32 [8], P(('grp', 'tp')), parts along dimension 0, may hold values from 0 to 4095
- in_gain: float32 [4096], replicated, may hold values from 0.1 to 1.9
- w_latent: bfloat16 [4096, 1024], P('sp'), may hold values from -0.09375 to 0.09375
- w_rope_key: bfloat16 [4096, 32], replicated, may hold values from -0.09375 to 0.09375
- kv_gain: float32 [1024], replicated, may hold values from 0.1 to 1.9
- w_up_key: bfloat16 [1024, 2048], P(None, 'tp'), may hold values from -0.1875 to 0.1875
- w_up_value: bfloat16 [1024, 2048], P(None, 'tp'), may hold values from -0.1875 to 0.1875
- q_nope: bfloat16 [8, 2048], P(('grp', 'sp'), 'tp'), parts along dimension 0, may hold values from -300 to 300, as said below
- q_rope: bfloat16 [8, 1024], P(('grp', 'sp'), 'tp'), parts along dimension 0, may hold values from -16 to 16
Outputs:
- keys: bfloat16 [8, 1024, 2048], P(('grp', 'sp'), None, 'tp'), parts along dimension 0
- values: bfloat16 [8, 1024, 2048], P(('grp', 'sp'), None, 'tp'), parts along dimension 0
- rope_keys: bfloat16 [8, 32, 1024], P(('grp', 'sp')), parts along dimension 0
- read: bfloat16 [8, 2048], P(('grp', 'sp'), 'tp'), parts along dimension 0
There are 2 independent parts, one for each index of `grp`. A program takes and returns all parts, laid end to end along the dimension named above; an argument that names none is the same for every part. Nothing has to cross between parts.
Inputs may be any that keep to these rules, and one draw needn't show every extreme that they name: `tokens`: entries of the layer's input. `q_nope`: entries of the first decoding token's queries.
All inputs are finite; a program needn't handle non-finite values.
Results may differ from a plain program's by a relative error of at most 0.02.
Values may be sent and summed in bfloat16 or wider, within the bound.
No kernel may reach another device: no remote copies, remote signals or barrier semaphores. Data moves between devices by JAX's collectives and lax.ppermute only.
A program may use at most 128 MiB of HBM per device.

v0:
```python
import jax
import jax.numpy as jnp
from jax import lax
from jax.sharding import PartitionSpec as P

HEAD = 64
ROPE = 32


EPS = 1e-06


def rms_scale(values, gain):
    wide = values.astype(jnp.float32)
    return wide * lax.rsqrt(jnp.mean(wide * wide, axis=-1, keepdims=True) + EPS) * gain


def rotate(raw, position):
    inverse = 10000.0 ** (-jnp.arange(0, ROPE, 2).astype(jnp.float32) / ROPE)
    angle = position.astype(jnp.float32)[..., None] * inverse
    cosine, sine = (jnp.cos(angle), jnp.sin(angle))
    half = ROPE // 2
    first, second = (raw[..., :half], raw[..., half:])
    return jnp.concatenate(
        [first * cosine - second * sine, second * cosine + first * sine], axis=-1
    )


def local(
    tokens, offsets, in_gain, w_latent, w_rope_key, kv_gain, w_up_key, w_up_value, q_nope, q_rope
):
    prompts, rows, width = tokens.shape
    n_sp = lax.axis_size("sp")
    length = n_sp * rows
    block = lax.axis_index("sp")
    normed = rms_scale(tokens.reshape(prompts * rows, width), in_gain).astype(jnp.bfloat16)
    latent_raw = jnp.dot(
        normed,
        lax.all_gather(w_latent, "sp", axis=0, tiled=True),
        preferred_element_type=jnp.float32,
    )
    latent = rms_scale(latent_raw, kv_gain).astype(jnp.bfloat16)
    position = offsets[:, None] + block * rows + jnp.arange(rows, dtype=jnp.int32)[None, :]
    rope_raw = jnp.dot(normed, w_rope_key, preferred_element_type=jnp.float32).reshape(
        prompts, rows, ROPE
    )
    rotated = rotate(rope_raw, position).astype(jnp.bfloat16)
    head_cols = w_up_key.shape[1]
    latent_every, rope_every = (
        lax.all_gather(latent.reshape(prompts, rows, latent.shape[1]), "tp", axis=0, tiled=True),
        lax.all_gather(rotated, "tp", axis=0, tiled=True),
    )
    latent_moved, rope_moved = (
        lax.all_to_all(latent_every[:, None], "sp", split_axis=0, concat_axis=1, tiled=True),
        lax.all_to_all(rope_every[:, None], "sp", split_axis=0, concat_axis=1, tiled=True),
    )
    latent_all = latent_moved.reshape(length, latent_moved.shape[3])
    rope_all = rope_moved.reshape(length, ROPE)
    keys = jnp.dot(latent_all, w_up_key, preferred_element_type=jnp.float32).astype(jnp.bfloat16)
    values = jnp.dot(latent_all, w_up_value, preferred_element_type=jnp.float32).astype(
        jnp.bfloat16
    )
    rope_keys = rope_all.T
    heads_here = head_cols // HEAD
    query = q_nope.reshape(heads_here, HEAD)
    rotary_q = q_rope.reshape(heads_here, ROPE)
    keys_split = keys.reshape(length, heads_here, HEAD)
    scores = jnp.einsum("hd,jhd->hj", query, keys_split, preferred_element_type=jnp.float32)
    scores = scores + jnp.dot(rotary_q, rope_keys, preferred_element_type=jnp.float32)
    scores = scores / jnp.sqrt(jnp.float32(HEAD + ROPE))
    peak = jnp.max(scores, axis=-1, keepdims=True)
    expo = jnp.exp(scores - peak)
    weights = (expo / jnp.sum(expo, axis=-1, keepdims=True)).astype(jnp.bfloat16)
    read = jnp.einsum(
        "hj,jhd->hd",
        weights,
        values.reshape(length, heads_here, HEAD),
        preferred_element_type=jnp.float32,
    )
    read = read.astype(jnp.bfloat16).reshape(1, heads_here * HEAD)
    return (keys[None], values[None], rope_keys[None], read)


def solution(mesh):
    in_specs = (
        P(("grp", "tp"), "sp", None),
        P(("grp", "tp")),
        P(),
        P("sp", None),
        P(),
        P(),
        P(None, "tp"),
        P(None, "tp"),
        P(("grp", "sp"), "tp"),
        P(("grp", "sp"), "tp"),
    )
    out_specs = (
        P(("grp", "sp"), None, "tp"),
        P(("grp", "sp"), None, "tp"),
        P(("grp", "sp"), None, None),
        P(("grp", "sp"), "tp"),
    )
    return jax.shard_map(local, mesh=mesh, in_specs=in_specs, out_specs=out_specs, check_vma=False)
```

profile of v0, /device:TPU:0, one launch (start us, length us, event | category | flops | bytes accessed | tf_op | source)
XLA Modules:
  0.0 260.1 jit_solution(4544893987934630213)
XLA Ops:
  7.2 0.0 copy-start
  7.2 0.0 all-gather.4.cloned.1.call-start
  7.2 0.7 all-gather.4.cloned.1.call-update
  7.9 0.0 all-gather.6.cloned.1.call-start
  8.0 0.9 copy-done.1
  8.9 0.5 fusion
  9.4 152.6 %all-gather.4.cloned.1.call-done = bf16[4096,1024]{1,0:T(8,128)(2,1)} async-done(((bf16[1024,1024]{1,0:T(8,128)(2,1)}), bf16[4096,1024]{1,0:T(8,128)(2,1)}) %all-gather.4.cloned.1.call-update) | async-done | bytes 8388624 | tf_op jit(solution)/shard_map/all_gather | solution.py:39
  161.9 5.9 %multiply_reduce_fusion = (f32[256]{0:T(256)S(1)}, f32[256,1024]{1,0:T(8,128)S(1)}) fusion(bf16[4096,1024]{1,0:T(8,128)(2,1)} %all-gather.4.cloned.1.call-done, bf16[1,256,4096]{2,1,0:T(8,128)(2,1)S(1)} %copy-done.1, f32[4096]{0:T(1024)S(1)} %copy-done.10, f32[256]{0:T(256)S(1)} %add_rsqrt_fusion.1), kind=kOutput, calls=%fused_computation.12 | convolution fusion | flops 2152201984 | bytes 11552768 | tf_op jit(solution)/shard_map/dot_general | solution.py:37
  167.8 0.9 multiply_convert_fusion
  168.8 0.0 all-gather.6.cloned.1.call-update
  169.5 0.8 convolution_bitcast_fusion.1
  170.3 0.1 fusion.16
  170.5 5.2 %all_gather.11 = bf16[4,256,32]{1,2,0:T(8,128)(2,1)S(1)} all-gather(bf16[1,256,32]{1,2,0:T(8,128)(2,1)S(1)} %pad_maximum_fusion), channel_id=1, replica_groups=mesh['grp'=2,'sp'=4,'tp'=4] {'tp'}, dimensions={0}, use_global_device_ids=true | all-gather | bytes 81920 | tf_op jit(solution)/shard_map/all_gather | solution.py:51
  175.7 8.1 %all_to_all.8 = bf16[4,1,256,32]{2,3,1,0:T(8,128)(2,1)S(1)} all-to-all(bf16[4,1,256,32]{2,3,1,0:T(8,128)(2,1)S(1)} %bitcast.64), channel_id=1, replica_groups=mesh['grp'=2,'sp'=4,'tp'=4] {'sp'}, dimensions={0} | all-to-all | bytes 131072 | tf_op jit(solution)/shard_map/all_to_all | solution.py:55
  183.8 5.9 %all-gather.6.cloned.1.call-done = bf16[1024,1024]{1,0:T(8,128)(2,1)} async-done(((bf16[256,1024]{1,0:T(8,128)(2,1)}), bf16[1024,1024]{1,0:T(8,128)(2,1)}) %all-gather.6.cloned.1.call-update) | async-done | bytes 2097168 | tf_op jit(solution)/shard_map/all_gather | solution.py:50
  189.7 4.7 %all-to-all-start = ((bf16[4,1,256,1024]{3,2,1,0:T(8,128)(2,1)}), bf16[4,1,256,1024]{3,2,1,0:T(8,128)(2,1)S(1)}, u32[]{:S(2)}, u32[]{:S(2)}) async-start(bf16[4,1,256,1024]{3,2,1,0:T(8,128)(2,1)} %bitcast.59), calls=%async_computation | async-start | bytes 4194304 | tf_op jit(solution)/shard_map/all_to_all | solution.py:54
  194.5 0.1 reshape.225
  194.6 0.1 reshape.214
  194.7 0.1 copy.21
  194.7 0.0 copy-start.4
  194.8 48.3 %all-to-all-done = bf16[4,1,256,1024]{3,2,1,0:T(8,128)(2,1)S(1)} async-done(((bf16[4,1,256,1024]{3,2,1,0:T(8,128)(2,1)}), bf16[4,1,256,1024]{3,2,1,0:T(8,128)(2,1)S(1)}, u32[]{:S(2)}, u32[]{:S(2)}) %all-to-all-start) | async-done | bytes 2097184 | tf_op jit(solution)/shard_map/all_to_all | solution.py:54
  243.0 1.3 copy-done.2
  244.4 3.0 %convolution_convert_fusion.1 = bf16[1024,512]{0,1:T(8,128)(2,1)S(1)} fusion(bf16[1024,1024]{1,0:T(8,128)(2,1)} %bitcast.60, bf16[1024,512]{1,0:T(8,128)(2,1)S(1)} %copy-done), kind=kOutput, calls=%fused_computation.6 | convolution fusion | flops 1074266112 | bytes 4194304 | tf_op jit(solution)/shard_map/dot_general | solution.py:59
  247.4 0.2 fusion.21
  247.7 0.2 fusion.20
  247.9 0.2 fusion.10
  248.1 0.1 fusion.19
  248.2 1.3 convolution_convert_fusion
  249.5 0.4 fusion.8
  249.9 0.7 reshape.216
  250.6 1.3 copy.22
  251.9 1.3 copy.23
  (27 shorter events, 0.1 us)
Async XLA Ops:
  7.2 237.2 %copy-start = (bf16[1024,512]{1,0:T(8,128)(2,1)S(1)}, bf16[1024,512]{1,0:T(8,128)(2,1)}, u32[]{:S(2)}) copy-start(bf16[1024,512]{1,0:T(8,128)(2,1)} %param.16) | copy-start | bytes 3145732
  7.2 1.7 copy-start.1
  7.2 154.8 %copy-start.10 = (f32[4096]{0:T(1024)S(1)}, f32[4096]{0:T(1024)}, u32[]{:S(2)}) copy-start(f32[4096]{0:T(1024)} %param.12) | copy-start | bytes 49156
  7.2 154.7 %all-gather.4.cloned.1.call-start = ((), (), s32[]{:S(2)}) async-start(), calls=%async_computation.2 | async-start | bytes 10485760 | tf_op jit(solution)/shard_map/all_gather | solution.py:39
  7.9 181.8 %all-gather.6.cloned.1.call-start = ((), (), s32[]{:S(2)}) async-start(), calls=%async_computation.3 | async-start | bytes 2621440 | tf_op jit(solution)/shard_map/all_gather | solution.py:50
  9.4 158.5 %copy-start.5 = (f32[1024]{0:T(1024)S(1)}, f32[1024]{0:T(1024)}, u32[]{:S(2)}) copy-start(f32[1024]{0:T(1024)} %param.15) | copy-start | bytes 12292
  167.8 1.7 copy-start.9
  189.7 4.7 %copy-start.6 = (bf16[1,512]{1,0:T(2,128)(2,1)S(1)}, bf16[1,512]{1,0:T(2,128)(2,1)}, u32[]{:S(2)}) copy-start(bf16[1,512]{1,0:T(2,128)(2,1)} %param.18) | copy-start | bytes 3076
  189.7 4.8 %copy-start.7 = (bf16[1,256]{1,0:T(2,128)(2,1)S(1)}, bf16[1,256]{1,0:T(2,128)(2,1)}, u32[]{:S(2)}) copy-start(bf16[1,256]{1,0:T(2,128)(2,1)} %param.19) | copy-start | bytes 1540
  189.7 53.3 %all-to-all-start = ((bf16[4,1,256,1024]{3,2,1,0:T(8,128)(2,1)}), bf16[4,1,256,1024]{3,2,1,0:T(8,128)(2,1)S(1)}, u32[]{:S(2)}, u32[]{:S(2)}) async-start(bf16[4,1,256,1024]{3,2,1,0:T(8,128)(2,1)} %bitcast.59), calls=%async_computation | async-start | bytes 4194304 | tf_op jit(solution)/shard_map/all_to_all | solution.py:54
  194.7 54.8 %copy-start.4 = (bf16[4,8,4,256]{3,1,2,0:T(8,128)(2,1)}, bf16[4,8,4,256]{3,1,2,0:T(8,128)(2,1)S(1)}, u32[]{:S(2)}) copy-start(bf16[4,8,4,256]{3,1,2,0:T(8,128)(2,1)S(1)} %copy.28) | copy-start | bytes 196612
  243.0 1.3 copy-start.2
  244.4 3.8 %copy-start.3 = (bf16[4,1,256,1024]{3,2,1,0:T(8,128)(2,1)S(1)}, bf16[4,1,256,1024]{3,2,1,0:T(8,128)(2,1)}, u32[]{:S(2)}) copy-start(bf16[4,1,256,1024]{3,2,1,0:T(8,128)(2,1)} %copy-done.2) | copy-start | bytes 6291460
  244.4 3.8 %copy-start.8 = (bf16[1024,512]{1,0:T(8,128)(2,1)S(1)}, bf16[1024,512]{1,0:T(8,128)(2,1)}, u32[]{:S(2)}) copy-start(bf16[1024,512]{1,0:T(8,128)(2,1)} %param.17) | copy-start | bytes 3145732
Sparse Core Ops, SparseCore 0:
  9.6 152.3 all-gather.3
  168.9 20.7 all-gather.5
where the time goes:
time: 260 us
  waiting for transfers between devices  207 us (80%)
  between operations  14.9 us (6%)
  blocking collectives  13.3 us (5%)
  matrix products  11.8 us (5%)
  local copies, waits for them, and re-layouts  5.8 us (2%)
  starting transfers between devices  4.81 us (2%)
    all_gather x1, waiting for transfers between devices, local(): lax.all_gather(w_latent, 'sp', axis=0, tiled=True)  153 us
    all_to_all x1, waiting for transfers between devices, local(): lax.all_to_all(latent_every[:, None], 'sp', split_axis=0, concat_axis=1,...  48.3 us
    all_to_all x1, blocking collectives, local(): lax.all_to_all(rope_every[:, None], 'sp', split_axis=0, concat_axis=1, ti...  8.1 us
    all_gather x1, waiting for transfers between devices, local(): lax.all_gather(latent.reshape(prompts, rows, latent.shape[1]), 'tp', axis...  5.92 us
    dot_general x1, matrix products, local(): jnp.dot(normed, lax.all_gather(w_latent, 'sp', axis=0, tiled=True), prefe...  5.85 us
    all_gather x1, blocking collectives, local(): lax.all_gather(rotated, 'tp', axis=0, tiled=True)  5.24 us
  transfers between devices with their start and end apart: 3, of which 3 were waited for; matrix products, arithmetic and copies ran while one was open for 1% of the time, Pallas kernels for 0%

commit v1 on v0

v1 whole, which is shorter than its diff:
```python
import jax
import jax.numpy as jnp
import numpy as np
from jax import lax
from jax.experimental import pallas as pl
from jax.experimental.pallas import tpu as pltpu
from jax.sharding import PartitionSpec as P


HEAD = 64
ROPE = 32


EPS = 1e-06


def rms_scale(values, gain):
    wide = values.astype(jnp.float32)
    return wide * lax.rsqrt(jnp.mean(wide * wide, axis=-1, keepdims=True) + EPS) * gain


def rotate(raw, position):
    inverse = 10000.0 ** (-jnp.arange(0, ROPE, 2).astype(jnp.float32) / ROPE)
    angle = position.astype(jnp.float32)[..., None] * inverse
    cosine, sine = (jnp.cos(angle), jnp.sin(angle))
    half = ROPE // 2
    first, second = (raw[..., :half], raw[..., half:])
    return jnp.concatenate(
        [first * cosine - second * sine, second * cosine + first * sine], axis=-1
    )


def rotate_first(raw, position):
    inverse = 10000.0 ** (-jnp.arange(0, ROPE, 2).astype(jnp.float32) / ROPE)
    angle = position.astype(jnp.float32)[None] * inverse[:, None, None]
    cosine, sine = (jnp.cos(angle), jnp.sin(angle))
    half = ROPE // 2
    first, second = (raw[:half], raw[half:])
    return jnp.concatenate(
        [first * cosine - second * sine, second * cosine + first * sine], axis=0
    )


def attend(keys, values, rope_keys, q_nope, q_rope):
    length, head_cols = keys.shape
    heads_here = head_cols // HEAD
    query = q_nope.reshape(heads_here, HEAD)
    rotary_q = q_rope.reshape(heads_here, ROPE)
    keys_split = keys.reshape(length, heads_here, HEAD)
    scores = jnp.einsum("hd,jhd->hj", query, keys_split, preferred_element_type=jnp.float32)
    scores = scores + jnp.dot(rotary_q, rope_keys, preferred_element_type=jnp.float32)
    scores = scores / jnp.sqrt(jnp.float32(HEAD + ROPE))
    peak = jnp.max(scores, axis=-1, keepdims=True)
    expo = jnp.exp(scores - peak)
    weights = (expo / jnp.sum(expo, axis=-1, keepdims=True)).astype(jnp.bfloat16)
    read = jnp.einsum(
        "hj,jhd->hd",
        weights,
        values.reshape(length, heads_here, HEAD),
        preferred_element_type=jnp.float32,
    )
    return read.astype(jnp.bfloat16).reshape(1, heads_here * HEAD)


def swap(value, axis, bits):
    n = lax.axis_size(axis)
    return lax.ppermute(value, axis, [(i, i ^ bits) for i in range(n)])


class Table:
    def __init__(self, scalars):
        self.scalars = scalars
        self.rows = []
        self.more = []

    def add(self, more=0, **terms):
        self.rows.append(terms)
        self.more.append(more)
        return len(self.rows) - 1

    def build(self):
        total = jnp.asarray(np.array(self.more, np.int32))
        for name, scalar in self.scalars.items():
            number = np.array([row.get(name, (0, 0))[0] for row in self.rows], np.int32)
            factor = np.array([row.get(name, (0, 0))[1] for row in self.rows], np.int32)
            total = total + (scalar.astype(jnp.int32) ^ number) * factor
        return total


def spread(
    tokens, offsets, in_gain, w_latent, w_rope_key, kv_gain, w_up_key, w_up_value, q_nope, q_rope
):
    prompts, rows, width = tokens.shape
    n_sp, n_tp, n_grp = (lax.axis_size("sp"), lax.axis_size("tp"), lax.axis_size("grp"))
    n_x = n_tp // 2
    z, t, y = (lax.axis_index("sp"), lax.axis_index("tp"), lax.axis_index("grp"))
    x, c = (t // 2, t % 2)
    rank = w_latent.shape[1]
    half = rank // 2
    k_block = w_latent.shape[0]
    own = prompts * rows
    per_chip = 2 * prompts
    sub = rows // n_x

    piece = k_block // n_grp // n_x
    mine = []
    source = w_latent
    for a in range(n_x):
        mine.append(
            lax.dynamic_slice(source, ((y * n_x + (x ^ a)) * piece, c * half), (piece, half))
        )
        source, mine[a] = lax.optimization_barrier((source, mine[a]))
    base = {(i, a): swap(mine[a], "sp", i) for i, a in fetches(n_sp, n_x)}
    corner = (n_sp - 1, 0)
    weights = {}
    for i, a in base:
        for g in range(n_grp):
            weights[i, a, 0, g] = swap(base[i, a], "grp", g) if g else base[i, a]
            if (i, a) == corner:
                for j in range(1, n_x):
                    weights[i, a, j, g] = swap(weights[i, a, 0, g], "tp", 2 * j)

    normed = lax.optimization_barrier(
        rms_scale(tokens.reshape(own, width), in_gain).astype(jnp.bfloat16)
    )
    shares = normed.reshape(prompts, n_x, sub, width)
    came = {}
    for j in range(1, n_x):
        share = lax.dynamic_index_in_dim(shares, x ^ j, 1, keepdims=False).reshape(-1, width)
        came[j] = swap(share, "tp", 2 * j)
    taken = []
    for s in range(2):
        taken.append(swap(normed, "tp", 1) if s else normed)
        taken += [swap(came[j], "tp", 1) if s else came[j] for j in range(1, n_x)]

    position = offsets[:, None] + z * rows + jnp.arange(rows, dtype=jnp.int32)[None, :]
    rope_raw = lax.dot_general(
        w_rope_key, normed, (((0,), (1,)), ((), ())), preferred_element_type=jnp.float32
    ).reshape(ROPE, prompts, rows)
    rotated = rotate_first(rope_raw, position).astype(jnp.bfloat16).transpose(1, 0, 2)
    moved = []
    for r in range(prompts):
        turn = lambda s: (r + s) % prompts
        send = lax.dynamic_index_in_dim(rotated, turn(z), 0, keepdims=False)
        moved.append(
            lax.ppermute(
                send,
                ("sp", "tp"),
                [
                    (s * n_tp + u, (prompts * u + turn(s)) * n_tp + s // prompts)
                    for s in range(n_sp)
                    for u in range(n_tp)
                ],
            )
        )
    moved = jnp.stack(moved)
    if prompts > 1:
        moved = jnp.concatenate(
            [
                lax.dynamic_index_in_dim(moved, (z - s) % prompts, 0, keepdims=True)
                for s in range(prompts)
            ],
            axis=0,
        )
    ropes = moved[None]
    for b in range(n_tp.bit_length() - 1):
        ropes = jnp.concatenate([ropes, swap(ropes, "tp", 1 << b)], axis=0)
    rope_keys = jnp.concatenate(
        [
            lax.dynamic_index_in_dim(ropes, u ^ t, 0, keepdims=False)[p]
            for u in range(n_tp)
            for p in range(prompts)
        ],
        axis=1,
    )

    table = Table(
        {
            "z": z,
            "x": x,
            "y": y,
            "c": c,
            "prompt_x": (z // per_chip) ^ x,
            "prompt_c": (z // prompts % 2) ^ c,
            "prompt": z % prompts,
        }
    )
    at_c = table.add(c=(0, 1))
    at_half = [table.add(c=(s, half)) for s in range(2)]
    at_keep = [table.add(x=(0, sub), more=p * rows) for p in range(prompts)]
    at_send = [
        table.add(
            prompt_c=(i // prompts % 2, n_x * prompts * sub),
            prompt_x=(i // per_chip, prompts * sub),
            prompt=(i % prompts, sub),
        )
        for i in range(n_sp)
    ]
    at_place = {
        (j, i): table.add(z=(i, rows), x=(j, sub)) for j in range(n_x) for i in range(n_sp)
    }
    at_piece = {(0, 0, 0, 0): table.add(z=(0, k_block))}
    for i, a, j, g in weights:
        at_piece[i, a, j, g] = table.add(
            z=(i, k_block), y=(g, n_x * piece), x=(a ^ j, piece)
        )
    stages = [stage for stage in stages_of(n_sp, n_x, n_grp) if stage]
    numbers = table.build()
    gain = kv_gain[None, :]
    latent = None
    for k, stage in enumerate(stages):
        latent = latent_part(
            numbers,
            (at_c, at_half, at_keep, at_send, at_piece),
            taken,
            w_latent if k == 0 else None,
            [(weights[one], one) for one in stage],
            latent,
            gain if k == len(stages) - 1 else None,
            prompts,
            sub,
            c,
        )
    blocks = {}
    for i in range(n_sp):
        blocks[0, 0, i] = swap(latent[i], "sp", i) if i else latent[0]
        for j in range(1, n_x):
            blocks[0, j, i] = swap(blocks[0, 0, i], "tp", 2 * j)
        for j in range(n_x):
            blocks[1, j, i] = swap(blocks[0, j, i], "tp", 1)
    cut = n_sp // 2
    caches = None
    for low, high in ((0, cut), (cut, n_sp)):
        if low < high:
            caches = final(
                numbers,
                (at_half, at_place),
                {key: block for key, block in blocks.items() if low <= key[2] < high},
                caches,
                (gain, w_up_key, w_up_value, rope_keys, q_nope, q_rope),
                n_sp * rows,
                high == n_sp,
            )
    keys, values, read = caches
    return (keys[None], values[None], rope_keys[None], read)


def fetches(n_sp, n_x):
    if n_sp == 2:
        return [(1, 0)]
    order = [(n_sp - 1, 0), (1, 0)]
    for i in range(2, n_sp - 1):
        order += [(i, a) for a in range(n_x - 1)]
    order += [(1, a) for a in range(1, n_x)]
    return order + [(i, n_x - 1) for i in range(2, n_sp - 1)]


def stages_of(n_sp, n_x, n_grp):
    order = fetches(n_sp, n_x)
    (early, late) = (order[:2], order[2:])
    first = [(i, a, 0, g) for i, a in early for g in range(n_grp)]
    first += [(*one, 0, 0) for one in late[: 1 + n_x]]
    done = set(first)
    rest = [(*one, 0, g) for one in late for g in range(n_grp) if (*one, 0, g) not in done]
    rest += [(*order[0], j, g) for g in range(n_grp) for j in range(1, n_x)]
    return [first, rest]


def latent_part(numbers, at, taken, w_own, pieces, start, gain, prompts, sub, c):
    at_c, at_half, at_keep, at_send, at_piece = at
    n_x = len(taken) // 2
    share = prompts * sub
    own = share * n_x
    kind = taken[0].dtype
    cols = pieces[0][0].shape[1]
    spans = [(at_piece[one], w.shape[0]) for w, one in pieces]
    if w_own is not None:
        spans = [(at_piece[0, 0, 0, 0], w_own.shape[0])] + spans
    depth = sum(size for _, size in spans)
    n_out = len(at_send)
    if any(size % 128 for _, size in spans):
        total = 0.0 if start is None else start
        rows = []
        for q, source in enumerate(taken):
            if q % n_x:
                rows.append(source)
            else:
                rows += [lax.dynamic_slice_in_dim(source, numbers[k], sub, 0) for k in at_keep]
        rows = jnp.concatenate(rows, axis=0)
        picked = [lax.dynamic_slice(rows, (0, numbers[k]), (2 * own, size)) for k, size in spans]
        held = [w for w, _ in pieces]
        if w_own is not None:
            held = [lax.dynamic_slice(w_own, (0, c * cols), (w_own.shape[0], cols))] + held
        total = total + jnp.dot(
            jnp.concatenate(picked, axis=1),
            jnp.concatenate(held, axis=0),
            preferred_element_type=jnp.float32,
        )
        if gain is None:
            return total
        total = (total * lax.dynamic_slice(gain, (0, c * cols), (1, cols))).astype(jnp.bfloat16)
        return [lax.dynamic_slice(total, (numbers[k], 0), (sub, cols)) for k in at_send]

    count = len(pieces)
    n_copies = len(spans) * (2 * (prompts + n_x - 1) + 1) + 1

    def kernel(numbers, *refs):
        refs = list(refs)

        def take(n):
            head = refs[:n]
            del refs[:n]
            return head

        sources = take(len(taken))
        weights = take(count)
        weights_own = take(1) if w_own is not None else None
        first = take(1) if start is not None else None
        scale = take(1) if gain is not None else None
        outs = take(1 if gain is None else n_out)
        rows, weight, *spare, sems = refs
        copies = []

        def copy(source, target):
            copies.append(pltpu.make_async_copy(source, target, sems.at[len(copies)]))

        groups = []
        column = 0
        held = (weights_own or []) + weights
        for q, (k, size) in enumerate(spans):
            before = len(copies)
            place = pl.multiple_of(numbers[k], 128)
            row = 0
            for n, source in enumerate(sources):
                starts = [0] if n % n_x else [pl.multiple_of(numbers[k], 8) for k in at_keep]
                many = share // len(starts)
                for low in starts:
                    copy(
                        source.at[pl.ds(low, many), pl.ds(place, size)],
                        rows.at[pl.ds(row, many), pl.ds(column, size)],
                    )
                    row += many
            source = held[q]
            if q == 0 and weights_own is not None:
                source = source.at[:, pl.ds(pl.multiple_of(numbers[at_half[0]], 128), cols)]
            copy(source, weight.at[pl.ds(column, size)])
            new = copies[before:]
            if groups and groups[-1][1] - groups[-1][0] + size <= 1024:
                groups[-1] = (groups[-1][0], column + size, groups[-1][2] + new)
            else:
                groups.append((column, column + size, new))
            column += size
        if first is not None:
            copy(first[0], spare[-1])
        for one in copies:
            one.start()
        total = None
        for low, high, some in groups:
            for one in some:
                one.wait()
            part = jnp.dot(
                rows[:, low:high], weight[low:high, :], preferred_element_type=jnp.float32
            )
            total = part if total is None else total + part
        if first is not None:
            copies[-1].wait()
            total = total + spare[-1][...]
        if scale is None:
            outs[0][...] = total
        else:
            side = numbers[at_c] == 0
            here = jnp.where(side, scale[0][:, :cols], scale[0][:, cols:])
            spare[0][...] = (total * here).astype(jnp.bfloat16)
            for i in range(n_out):
                outs[i][...] = spare[0][pl.ds(pl.multiple_of(numbers[at_send[i]], sub), sub), :]

    whole = pl.BlockSpec(memory_space=pltpu.VMEM)
    smem = pl.BlockSpec(memory_space=pltpu.SMEM)
    hbm = pl.BlockSpec(memory_space=pl.ANY)
    operands = list(taken) + [w for w, _ in pieces] + ([w_own] if w_own is not None else [])
    kinds = [hbm] * len(operands) + ([hbm] if start is not None else [])
    kinds += [whole] if gain is not None else []
    extra = ([start] if start is not None else []) + ([gain] if gain is not None else [])
    if gain is None:
        out = (jax.ShapeDtypeStruct((2 * own, cols), jnp.float32),)
        spare = []
    else:
        out = (jax.ShapeDtypeStruct((sub, cols), jnp.bfloat16),) * n_out
        spare = [pltpu.VMEM((2 * own, cols), jnp.bfloat16)]
    if start is not None:
        spare = spare + [pltpu.VMEM((2 * own, cols), jnp.float32)]
    result = pl.pallas_call(
        kernel,
        out_shape=out,
        in_specs=[smem] + kinds,
        out_specs=(whole,) * len(out),
        scratch_shapes=[pltpu.VMEM((2 * own, depth), kind), pltpu.VMEM((depth, cols), kind)]
        + spare
        + [pltpu.SemaphoreType.DMA((n_copies,))],
        cost_estimate=pl.CostEstimate(
            flops=4 * own * cols * depth, bytes_accessed=4 * own * depth, transcendentals=0
        ),
    )(numbers, *operands, *extra)
    return result[0] if gain is None else result


def final(numbers, at, blocks, caches, others, length, last):
    at_half, at_place = at
    gain, w_up_key, w_up_value, rope_keys, q_nope, q_rope = others
    rank, head_cols = w_up_key.shape
    heads = head_cols // HEAD
    cols = rank // 2
    sub = next(iter(blocks.values())).shape[0]
    here = sorted({key[1:] for key in blocks})
    before = [key for key in sorted(at_place) if key not in here] if caches is not None else []
    n_rows = len(here) * sub
    names = sorted(blocks)

    def kernel(numbers, *refs):
        refs = list(refs)

        def take(n):
            head = refs[:n]
            del refs[:n]
            return head

        gain, up_key, up_value = take(3)
        rope, query, rotary = take(3) if last else (None, None, None)
        pieces = dict(zip(names, take(len(names))))
        old = take(2) if caches is not None else None
        out_k, out_v = take(2)
        read = take(1)[0] if last else None
        latent, wk, wv, keys, values, sems = refs
        copies = []

        def copy(source, target):
            one = pltpu.make_async_copy(source, target, sems.at[len(copies)])
            copies.append(one)
            one.start()
            return one

        loads = []
        for k, key in enumerate(here):
            for s in range(2):
                loads.append(
                    copy(
                        pieces[(s, *key)],
                        latent.at[
                            pl.ds(k * sub, sub),
                            pl.ds(pl.multiple_of(numbers[at_half[s]], 128), cols),
                        ],
                    )
                )
        load_k = copy(up_key, wk)
        load_v = copy(up_value, wv)
        known = []
        if last:
            for key in before:
                place = pl.ds(pl.multiple_of(numbers[at_place[key]], sub), sub)
                known.append(copy(out_k.at[place], keys.at[place]))
                known.append(copy(out_v.at[place], values.at[place]))
        inverse = 1.0 / gain[...]
        for one in loads:
            one.wait()
        stores = []
        factors = []
        for weight, load, cache, out in (
            (wk, load_k, keys, out_k),
            (wv, load_v, values, out_v),
        ):
            load.wait()
            for k in range(0, len(here), 2):
                group = here[k : k + 2]
                rows = latent[k * sub : (k + len(group)) * sub, :]
                if load is load_k:
                    plain = rows.astype(jnp.float32) * inverse
                    squares = jnp.sum(plain * plain, axis=1, keepdims=True)
                    factors.append(lax.rsqrt(squares / rank + EPS))
                got = jnp.dot(rows, weight[...], preferred_element_type=jnp.float32)
                got = (got * factors[k // 2]).astype(cache.dtype)
                for q, key in enumerate(group):
                    place = pl.ds(pl.multiple_of(numbers[at_place[key]], sub), sub)
                    cache[place, :] = got[q * sub : (q + 1) * sub, :]
                    stores.append(copy(cache.at[place], out.at[place]))
        if last:
            for one in known:
                one.wait()

            def apart(flat, width):
                head = lax.broadcasted_iota(jnp.int32, (heads, heads * width), 0)
                column = lax.broadcasted_iota(jnp.int32, (heads, heads * width), 1)
                return jnp.where(column // width == head, flat.astype(jnp.float32), 0.0)

            fold = lax.broadcasted_iota(jnp.int32, (heads * ROPE, ROPE), 0) % ROPE
            fold = fold == lax.broadcasted_iota(jnp.int32, (heads * ROPE, ROPE), 1)
            turned = jnp.dot(
                apart(rotary[...], ROPE).astype(jnp.bfloat16),
                fold.astype(jnp.float32).astype(jnp.bfloat16),
                preferred_element_type=jnp.float32,
            ).astype(jnp.bfloat16)
            scores = lax.dot_general(
                apart(query[...], HEAD).astype(jnp.bfloat16),
                keys[...],
                (((1,), (1,)), ((), ())),
                preferred_element_type=jnp.float32,
            )
            scores = scores + jnp.dot(turned, rope[...], preferred_element_type=jnp.float32)
            scores = scores / jnp.sqrt(jnp.float32(HEAD + ROPE))
            expo = jnp.exp(scores - jnp.max(scores, axis=-1, keepdims=True))
            weights = (expo / jnp.sum(expo, axis=-1, keepdims=True)).astype(jnp.bfloat16)
            mixed = jnp.dot(weights, values[...], preferred_element_type=jnp.float32)
            head = lax.broadcasted_iota(jnp.int32, (heads, head_cols), 0)
            column = lax.broadcasted_iota(jnp.int32, (heads, head_cols), 1)
            mixed = jnp.where(column // HEAD == head, mixed, 0.0)
            read[...] = jnp.sum(mixed, axis=0, keepdims=True).astype(read.dtype)
        for one in stores:
            one.wait()

    whole = pl.BlockSpec(memory_space=pltpu.VMEM)
    smem = pl.BlockSpec(memory_space=pltpu.SMEM)
    hbm = pl.BlockSpec(memory_space=pl.ANY)
    cache = jax.ShapeDtypeStruct((length, head_cols), jnp.bfloat16)
    out = [cache, cache]
    specs = [hbm, hbm]
    operands = [gain, w_up_key, w_up_value]
    kinds = [whole, hbm, hbm]
    if last:
        out.append(jax.ShapeDtypeStruct((1, head_cols), jnp.bfloat16))
        specs.append(whole)
        operands += [rope_keys, q_nope, q_rope]
        kinds += [whole] * 3
    operands += [blocks[name] for name in names]
    kinds += [hbm] * len(names)
    aliases = {}
    if caches is not None:
        aliases = {1 + len(operands): 0, 2 + len(operands): 1}
        operands += list(caches[:2])
        kinds += [hbm, hbm]
    return pl.pallas_call(
        kernel,
        out_shape=tuple(out),
        in_specs=[smem] + kinds,
        out_specs=tuple(specs),
        input_output_aliases=aliases,
        scratch_shapes=[
            pltpu.VMEM((n_rows, rank), jnp.bfloat16),
            pltpu.VMEM((rank, head_cols), w_up_key.dtype),
            pltpu.VMEM((rank, head_cols), w_up_key.dtype),
            pltpu.VMEM((length, head_cols), jnp.bfloat16),
            pltpu.VMEM((length, head_cols), jnp.bfloat16),
            pltpu.SemaphoreType.DMA((4 * len(here) + 2 * len(before) + 2,)),
        ],
        cost_estimate=pl.CostEstimate(
            flops=4 * n_rows * rank * head_cols, bytes_accessed=8 * rank * head_cols, transcendentals=0
        ),
    )(numbers, *operands)


def gathered(
    tokens, offsets, in_gain, w_latent, w_rope_key, kv_gain, w_up_key, w_up_value, q_nope, q_rope
):
    prompts, rows, width = tokens.shape
    n_sp = lax.axis_size("sp")
    length = n_sp * rows
    block = lax.axis_index("sp")
    normed = rms_scale(tokens.reshape(prompts * rows, width), in_gain).astype(jnp.bfloat16)
    latent_raw = jnp.dot(
        normed,
        lax.all_gather(w_latent, "sp", axis=0, tiled=True),
        preferred_element_type=jnp.float32,
    )
    latent = rms_scale(latent_raw, kv_gain).astype(jnp.bfloat16)
    position = offsets[:, None] + block * rows + jnp.arange(rows, dtype=jnp.int32)[None, :]
    rope_raw = jnp.dot(normed, w_rope_key, preferred_element_type=jnp.float32).reshape(
        prompts, rows, ROPE
    )
    rotated = rotate(rope_raw, position).astype(jnp.bfloat16)
    latent_every, rope_every = (
        lax.all_gather(latent.reshape(prompts, rows, latent.shape[1]), "tp", axis=0, tiled=True),
        lax.all_gather(rotated, "tp", axis=0, tiled=True),
    )
    latent_moved, rope_moved = (
        lax.all_to_all(latent_every[:, None], "sp", split_axis=0, concat_axis=1, tiled=True),
        lax.all_to_all(rope_every[:, None], "sp", split_axis=0, concat_axis=1, tiled=True),
    )
    latent_all = latent_moved.reshape(length, latent_moved.shape[3])
    keys = jnp.dot(latent_all, w_up_key, preferred_element_type=jnp.float32).astype(jnp.bfloat16)
    values = jnp.dot(latent_all, w_up_value, preferred_element_type=jnp.float32).astype(
        jnp.bfloat16
    )
    rope_keys = rope_moved.reshape(length, ROPE).T
    read = attend(keys, values, rope_keys, q_nope, q_rope)
    return (keys[None], values[None], rope_keys[None], read)


def local(tokens, *rest):
    prompts, rows, _ = tokens.shape
    n_sp, n_tp, n_grp = (lax.axis_size("sp"), lax.axis_size("tp"), lax.axis_size("grp"))
    w_latent = rest[2]
    twos = all(n & (n - 1) == 0 for n in (n_sp, n_tp, n_grp))
    if (
        twos
        and n_tp > 1
        and n_sp == prompts * n_tp
        and rows % (n_tp // 2) == 0
        and w_latent.shape[0] % (n_tp // 2 * n_grp * 2) == 0
        and w_latent.shape[1] % 2 == 0
    ):
        return spread(tokens, *rest)
    return gathered(tokens, *rest)


def solution(mesh):
    in_specs = (
        P(("grp", "tp"), "sp", None),
        P(("grp", "tp")),
        P(),
        P("sp", None),
        P(),
        P(),
        P(None, "tp"),
        P(None, "tp"),
        P(("grp", "sp"), "tp"),
        P(("grp", "sp"), "tp"),
    )
    out_specs = (
        P(("grp", "sp"), None, "tp"),
        P(("grp", "sp"), None, "tp"),
        P(("grp", "sp"), None, None),
        P(("grp", "sp"), "tp"),
    )

    return jax.shard_map(local, mesh=mesh, in_specs=in_specs, out_specs=out_specs, check_vma=False)
```

time: 260 us -> 131 us (0.50)
  waiting for transfers between devices: 207 us -> 47.4 us
  starting transfers between devices: 4.81 us -> 48.4 us
  Pallas kernels: 0 us -> 20.8 us
  blocking collectives: 13.3 us -> 0 us
  between operations: 14.9 us -> 1.88 us
  matrix products: 11.8 us -> 0.72 us
    all_gather x2 -> x0, waiting for transfers between devices: 158 us -> none  [the longest x1 153 us: local(): lax.all_gather(w_latent, 'sp', axis=0, tiled=True)]
    ppermute x0 -> x33, starting transfers between devices: none -> 48.4 us  [the longest x32 47.7 us: swap(): return lax.ppermute(value, axis, [(i, i ^ bits) for i in range(n)])]
    all_to_all x1 -> x0, waiting for transfers between devices: 48.3 us -> none  [local(): lax.all_to_all(latent_every[:, None], 'sp', split_axis=0, concat_axis=1,...]
    ppermute x0 -> x33, waiting for transfers between devices: none -> 47.4 us  [the longest x32 47.4 us: swap(): return lax.ppermute(value, axis, [(i, i ^ bits) for i in range(n)])]
    pallas_call x0 -> x4, Pallas kernels: none -> 20.8 us  [the longest x2 10.5 us: latent_part(): pl.pallas_call(kernel, out_shape=out, in_specs=[smem] + kinds, out_specs=...]
    dot_general x7 -> x1, matrix products: 11.8 us -> 0.72 us  [spread(): lax.dot_general(w_rope_key, normed, (((0,), (1,)), ((), ())), preferred_e...]
    all_to_all x1 -> x0, blocking collectives: 8.1 us -> none  [local(): lax.all_to_all(rope_every[:, None], 'sp', split_axis=0, concat_axis=1, ti...]
    all_gather x1 -> x0, blocking collectives: 5.24 us -> none  [local(): lax.all_gather(rotated, 'tp', axis=0, tiled=True)]
  transfers between devices with their start and end apart: 3 -> 33, of which waited for: 3 -> 11; matrix products, arithmetic and copies ran while one was open for 1% -> 4% of each run, Pallas kernels for 0% -> 12%
where the time goes in v1:
time: 131 us; the launch traced here: 130 us
  starting transfers between devices  48.4 us (37%)
  waiting for transfers between devices  47.4 us (36%)
  Pallas kernels  20.8 us (16%)
  local copies, waits for them, and re-layouts  6.75 us (5%)
  other arithmetic  4.34 us (3%)
  between operations  1.88 us (1%)
    ppermute x32, starting transfers between devices, swap(): return lax.ppermute(value, axis, [(i, i ^ bits) for i in range(n)])  47.7 us
    ppermute x32, waiting for transfers between devices, swap(): return lax.ppermute(value, axis, [(i, i ^ bits) for i in range(n)])  47.4 us
    pallas_call x2, Pallas kernels, latent_part(): pl.pallas_call(kernel, out_shape=out, in_specs=[smem] + kinds, out_specs=...  10.5 us
    pallas_call x2, Pallas kernels, final(): pl.pallas_call(kernel, out_shape=tuple(out), in_specs=[smem] + kinds, out...  10.3 us
    dynamic_slice x2, local copies, waits for them, and re-layouts, spread(): lax.dynamic_slice(source, ((y * n_x + (x ^ a)) * piece, c * half), (piece...  3.39 us
  transfers between devices with their start and end apart: 33, of which 11 were waited for; matrix products, arithmetic and copies ran while one was open for 4% of the time, Pallas kernels for 12%

profile of v1, /device:TPU:0, one launch (start us, length us, event | category | flops | bytes accessed | tf_op | source)
XLA Modules:
  0.0 130.3 jit_solution(12155294407460219752)
XLA Ops:
  0.7 2.2 %fusion = f32[256]{0:T(256)S(1)} fusion(bf16[1,256,4096]{2,1,0:T(8,128)(2,1)} %param.25), kind=kLoop, calls=%fused_computation.2 | loop fusion | flops 3145472 | bytes 2098176 | tf_op jit(solution)/shard_map/reduce_sum | solution.py:19
  3.6 1.2 dynamic-slice_bitcast_fusion
  4.9 3.0 %collective-permute-start.3 = (bf16[128,4096]{1,0:T(8,128)(2,1)}, bf16[128,4096]{1,0:T(8,128)(2,1)S(1)}, u32[]{:S(2)}, u32[]{:S(2)}) collective-permute-start(bf16[128,4096]{1,0:T(8,128)(2,1)} %dynamic-slice_bitcast_fusion), channel_id=1, source_target_pairs={{0,2},{1,3},{2,0},{3,1},{4,6},{5,7},{6,4},{7,5},{8,10},{9,11},{10,... | collective-permute-start | bytes 3145736 | tf_op jit(solution)/shard_map/ppermute | solution.py:67
  7.9 1.7 %dynamic_slice.30 = bf16[256,512]{1,0:T(8,128)(2,1)} dynamic-slice(bf16[1024,1024]{1,0:T(8,128)(2,1)} %refs_11_.1, s32[]{:T(128)S(6)} %select_n.61, s32[]{:T(128)S(6)} %select_n.62), dynamic_slice_sizes={256,512} | dynamic-slice | bytes 524292 | tf_op jit(solution)/shard_map/dynamic_slice | solution.py:110
  9.6 1.7 %dynamic_slice.31 = bf16[256,512]{1,0:T(8,128)(2,1)} dynamic-slice(bf16[1024,1024]{1,0:T(8,128)(2,1)} %refs_11_.1, s32[]{:T(128)S(6)} %select_n.63, s32[]{:T(128)S(6)} %select_n.62), dynamic_slice_sizes={256,512} | dynamic-slice | bytes 524292 | tf_op jit(solution)/shard_map/dynamic_slice | solution.py:110
  11.3 2.6 %collective-permute-start.10 = (bf16[256,512]{1,0:T(8,128)(2,1)}, bf16[256,512]{1,0:T(8,128)(2,1)}, u32[]{:S(2)}, u32[]{:S(2)}) collective-permute-start(bf16[256,512]{1,0:T(8,128)(2,1)} %dynamic_slice.31), channel_id=1, source_target_pairs={{0,8},{4,12},{8,0},{12,4},{1,9},{5,13},{9,1},{13,5},{2,10},{6,14},... | collective-permute-start | bytes 786440 | tf_op jit(solution)/shard_map/ppermute | solution.py:67
  14.6 16.6 %collective-permute-done.3.refs_1_ = bf16[128,4096]{1,0:T(8,128)(2,1)S(1)} collective-permute-done((bf16[128,4096]{1,0:T(8,128)(2,1)}, bf16[128,4096]{1,0:T(8,128)(2,1)S(1)}, u32[]{:S(2)}, u32[]{:S(2)}) %collective-permute-start.3) | collective-permute-done | bytes 1048608 | tf_op jit(solution)/shard_map/ppermute | solution.py:67
  32.8 4.8 %collective-permute-start.1 = (bf16[1,1,32,256]{3,2,1,0:T(8,128)(2,1)S(1)}, bf16[1,1,32,256]{3,2,1,0:T(8,128)(2,1)S(1)}, u32[]{:S(2)}, u32[]{:S(2)}) collective-permute-start(bf16[1,1,32,256]{3,2,1,0:T(8,128)(2,1)S(1)} %bitcast.32), channel_id=1, source_target_pairs={{0,1},{1,0},{2,3},{3,2},{4,5},{5,4},{6,7},{7,6},{8,9},{9,8},{10,11... | collective-permute-start | bytes 49160 | tf_op jit(solution)/shard_map/ppermute | solution.py:67
  37.7 1.4 %collective-permute-start.8 = (bf16[256,512]{1,0:T(8,128)(2,1)}, bf16[256,512]{1,0:T(8,128)(2,1)}, u32[]{:S(2)}, u32[]{:S(2)}) collective-permute-start(bf16[256,512]{1,0:T(8,128)(2,1)} %dynamic_slice.31), channel_id=1, source_target_pairs={{0,4},{4,0},{8,12},{12,8},{1,5},{5,1},{9,13},{13,9},{2,6},{6,2},{1... | collective-permute-start | bytes 786440 | tf_op jit(solution)/shard_map/ppermute | solution.py:67
  39.1 5.9 %collective-permute-start.12 = (bf16[256,512]{1,0:T(8,128)(2,1)}, bf16[256,512]{1,0:T(8,128)(2,1)}, u32[]{:S(2)}, u32[]{:S(2)}) collective-permute-start(bf16[256,512]{1,0:T(8,128)(2,1)} %dynamic_slice.30), channel_id=1, source_target_pairs={{0,12},{4,8},{8,4},{12,0},{1,13},{5,9},{9,5},{13,1},{2,14},{6,10},... | collective-permute-start | bytes 786440 | tf_op jit(solution)/shard_map/ppermute | solution.py:67
  45.0 1.6 %collective-permute-done.8.refs_9_ = bf16[256,512]{1,0:T(8,128)(2,1)} collective-permute-done((bf16[256,512]{1,0:T(8,128)(2,1)}, bf16[256,512]{1,0:T(8,128)(2,1)}, u32[]{:S(2)}, u32[]{:S(2)}) %collective-permute-start.8) | collective-permute-done | bytes 262176 | tf_op jit(solution)/shard_map/ppermute | solution.py:67
  46.5 10.5 %collective-permute-start.6 = (bf16[256,512]{1,0:T(8,128)(2,1)}, bf16[256,512]{1,0:T(8,128)(2,1)}, u32[]{:S(2)}, u32[]{:S(2)}) collective-permute-start(bf16[256,512]{1,0:T(8,128)(2,1)} %dynamic_slice.30), channel_id=1, source_target_pairs={{0,8},{4,12},{8,0},{12,4},{1,9},{5,13},{9,1},{13,5},{2,10},{6,14},... | collective-permute-start | bytes 786440 | tf_op jit(solution)/shard_map/ppermute | solution.py:67
  57.0 1.5 %collective-permute-start.14 = (bf16[256,512]{1,0:T(8,128)(2,1)}, bf16[256,512]{1,0:T(8,128)(2,1)}, u32[]{:S(2)}, u32[]{:S(2)}) collective-permute-start(bf16[256,512]{1,0:T(8,128)(2,1)} %collective-permute-done.12.refs_4_), channel_id=1, source_target_pairs={{0,16},{16,0},{1,17},{17,1},{2,18},{18,2},{3,19},{19,3},{4,20},{20... | collective-permute-start | bytes 786440 | tf_op jit(solution)/shard_map/ppermute | solution.py:67
  58.5 5.6 %collective-permute-done.16.refs_6_ = bf16[256,512]{1,0:T(8,128)(2,1)} collective-permute-done((bf16[256,512]{1,0:T(8,128)(2,1)}, bf16[256,512]{1,0:T(8,128)(2,1)}, u32[]{:S(2)}, u32[]{:S(2)}) %collective-permute-start.16) | collective-permute-done | bytes 262176 | tf_op jit(solution)/shard_map/ppermute | solution.py:67
  64.1 1.5 %collective-permute-start.17 = (bf16[256,512]{1,0:T(8,128)(2,1)}, bf16[256,512]{1,0:T(8,128)(2,1)}, u32[]{:S(2)}, u32[]{:S(2)}) collective-permute-start(bf16[256,512]{1,0:T(8,128)(2,1)} %collective-permute-done.16.refs_6_), channel_id=1, source_target_pairs={{0,16},{16,0},{1,17},{17,1},{2,18},{18,2},{3,19},{19,3},{4,20},{20... | collective-permute-start | bytes 786440 | tf_op jit(solution)/shard_map/ppermute | solution.py:67
  65.6 2.9 %collective-permute-done.6.refs_8_ = bf16[256,512]{1,0:T(8,128)(2,1)} collective-permute-done((bf16[256,512]{1,0:T(8,128)(2,1)}, bf16[256,512]{1,0:T(8,128)(2,1)}, u32[]{:S(2)}, u32[]{:S(2)}) %collective-permute-start.6) | collective-permute-done | bytes 262176 | tf_op jit(solution)/shard_map/ppermute | solution.py:67
  68.6 1.1 collective-permute-start.13
  69.7 1.5 %collective-permute-start.11 = (bf16[256,512]{1,0:T(8,128)(2,1)}, bf16[256,512]{1,0:T(8,128)(2,1)}, u32[]{:S(2)}, u32[]{:S(2)}) collective-permute-start(bf16[256,512]{1,0:T(8,128)(2,1)} %collective-permute-done.10.refs_10_), channel_id=1, source_target_pairs={{0,16},{16,0},{1,17},{17,1},{2,18},{18,2},{3,19},{19,3},{4,20},{20... | collective-permute-start | bytes 786440 | tf_op jit(solution)/shard_map/ppermute | solution.py:67
  71.2 2.4 %collective-permute-done.17.refs_7_ = bf16[256,512]{1,0:T(8,128)(2,1)} collective-permute-done((bf16[256,512]{1,0:T(8,128)(2,1)}, bf16[256,512]{1,0:T(8,128)(2,1)}, u32[]{:S(2)}, u32[]{:S(2)}) %collective-permute-start.17) | collective-permute-done | bytes 262176 | tf_op jit(solution)/shard_map/ppermute | solution.py:67
  73.6 1.5 %collective-permute-start.9 = (bf16[256,512]{1,0:T(8,128)(2,1)}, bf16[256,512]{1,0:T(8,128)(2,1)}, u32[]{:S(2)}, u32[]{:S(2)}) collective-permute-start(bf16[256,512]{1,0:T(8,128)(2,1)} %collective-permute-done.8.refs_9_), channel_id=1, source_target_pairs={{0,16},{16,0},{1,17},{17,1},{2,18},{18,2},{3,19},{19,3},{4,20},{20... | collective-permute-start | bytes 786440 | tf_op jit(solution)/shard_map/ppermute | solution.py:67
  77.1 5.9 %shard_map.264.refs_9_ = f32[512,512]{1,0:T(8,128)} custom-call(s32[29]{0:T(128)} %multiply_add_fusion.numbers, bf16[256,4096]{1,0:T(8,128)(2,1)} %copy-done.1, bf16[128,4096]{1,0:T(8,128)(2,1)} %copy-done.3, bf16[256,4096]{1,0:T(8,128)(2,1)} %collective-permute-done.4.refs_2_, bf16[128,4096]{1,0:T(8,128)(2,1)} %collective-permute-done.5.refs_3_, ...), custom_call_target="tpu_custom_call" | custom-call | flops 1476395008 | bytes 2883584 | tf_op jit(solution)/shard_map/pallas_call | solution.py:392
  83.0 1.3 %collective-permute-start.2 = (bf16[2,1,32,256]{3,2,1,0:T(8,128)(2,1)S(1)}, bf16[2,1,32,256]{3,2,1,0:T(8,128)(2,1)S(1)}, u32[]{:S(2)}, u32[]{:S(2)}) collective-permute-start(bf16[2,1,32,256]{3,2,1,0:T(8,128)(2,1)S(1)} %pad_maximum_fusion.2), channel_id=1, source_target_pairs={{0,2},{1,3},{2,0},{3,1},{4,6},{5,7},{6,4},{7,5},{8,10},{9,11},{10,... | collective-permute-start | bytes 98312 | tf_op jit(solution)/shard_map/ppermute | solution.py:67
  84.8 3.7 %collective-permute-done.7.refs_4_ = bf16[256,512]{1,0:T(8,128)(2,1)} collective-permute-done((bf16[256,512]{1,0:T(8,128)(2,1)}, bf16[256,512]{1,0:T(8,128)(2,1)}, u32[]{:S(2)}, u32[]{:S(2)}) %collective-permute-start.7) | collective-permute-done | bytes 262176 | tf_op jit(solution)/shard_map/ppermute | solution.py:67
  89.2 4.6 %shard_map.265 = (bf16[128,512]{1,0:T(8,128)(2,1)}, bf16[128,512]{1,0:T(8,128)(2,1)}, bf16[128,512]{1,0:T(8,128)(2,1)}, bf16[128,512]{1,0:T(8,128)(2,1)}) custom-call(s32[29]{0:T(128)} %multiply_add_fusion.numbers, bf16[256,4096]{1,0:T(8,128)(2,1)} %copy-done.1, bf16[128,4096]{1,0:T(8,128)(2,1)} %copy-done.3, ...), custom_call_target="tpu_custom_call" | custom-call | flops 671088640 | bytes 1310720 | tf_op jit(solution)/shard_map/pallas_call | solution.py:392
  94.8 1.7 %collective-permute-start.27 = (bf16[128,512]{1,0:T(8,128)(2,1)}, bf16[128,512]{1,0:T(8,128)(2,1)S(1)}, u32[]{:S(2)}, u32[]{:S(2)}) collective-permute-start(bf16[128,512]{1,0:T(8,128)(2,1)} %get-tuple-element.21.refs_3_), channel_id=1, source_target_pairs={{0,2},{1,3},{2,0},{3,1},{4,6},{5,7},{6,4},{7,5},{8,10},{9,11},{10,... | collective-permute-start | bytes 393224 | tf_op jit(solution)/shard_map/ppermute | solution.py:67
  96.5 3.4 %collective-permute-start.18 = (bf16[128,512]{1,0:T(8,128)(2,1)}, bf16[128,512]{1,0:T(8,128)(2,1)S(1)}, u32[]{:S(2)}, u32[]{:S(2)}) collective-permute-start(bf16[128,512]{1,0:T(8,128)(2,1)} %get-tuple-element.19), channel_id=1, source_target_pairs={{0,8},{4,12},{8,0},{12,4},{1,9},{5,13},{9,1},{13,5},{2,10},{6,14},... | collective-permute-start | bytes 393224 | tf_op jit(solution)/shard_map/ppermute | solution.py:67
  100.9 8.5 %collective-permute-done.18.refs_6_ = bf16[128,512]{1,0:T(8,128)(2,1)S(1)} collective-permute-done((bf16[128,512]{1,0:T(8,128)(2,1)}, bf16[128,512]{1,0:T(8,128)(2,1)S(1)}, u32[]{:S(2)}, u32[]{:S(2)}) %collective-permute-start.18) | collective-permute-done | bytes 131104 | tf_op jit(solution)/shard_map/ppermute | solution.py:67
  110.2 1.2 collective-permute-start.21
  112.2 3.5 %collective-permute-done.20.refs_8_ = bf16[128,512]{1,0:T(8,128)(2,1)S(1)} collective-permute-done((bf16[128,512]{1,0:T(8,128)(2,1)S(1)}, bf16[128,512]{1,0:T(8,128)(2,1)S(1)}, u32[]{:S(2)}, u32[]{:S(2)}) %collective-permute-start.20) | collective-permute-done | bytes 131104 | tf_op jit(solution)/shard_map/ppermute | solution.py:67
  115.8 1.9 %collective-permute-done.21.refs_9_ = bf16[128,512]{1,0:T(8,128)(2,1)S(1)} collective-permute-done((bf16[128,512]{1,0:T(8,128)(2,1)S(1)}, bf16[128,512]{1,0:T(8,128)(2,1)S(1)}, u32[]{:S(2)}, u32[]{:S(2)}) %collective-permute-start.21) | collective-permute-done | bytes 131104 | tf_op jit(solution)/shard_map/ppermute | solution.py:67
  119.1 4.6 %shard_map.266 = (bf16[1024,512]{1,0:T(8,128)(2,1)}, bf16[1024,512]{1,0:T(8,128)(2,1)}) custom-call(s32[29]{0:T(128)} %multiply_add_fusion.numbers, f32[1,1024]{1,0:T(1,128)} %bitcast.36, bf16[1024,512]{1,0:T(8,128)(2,1)} %refs_1_.3, bf16[1024,512]{1,0:T(8,128)(2,1)} %refs_2_.3, bf16[128,512]{1,0:T(8,128)(2,1)} %get-tuple-element.21.refs_3_, ...), custom_call_target="tpu_custom_call" | custom-call | flops 1073741824 | bytes 4194304 | tf_op jit(solution)/shard_map/pallas_call | solution.py:539
  124.5 5.7 %shard_map.267 = (bf16[1024,512]{1,0:T(8,128)(2,1)}, bf16[1024,512]{1,0:T(8,128)(2,1)}, bf16[1,512]{1,0:T(2,128)(2,1)}) custom-call(s32[29]{0:T(128)} %multiply_add_fusion.numbers, f32[1,1024]{1,0:T(1,128)} %bitcast.37, bf16[1024,512]{1,0:T(8,128)(2,1)} %refs_1_.3, bf16[1024,512]{1,0:T(8,128)(2,1)} %refs_2_.3, ...), custom_call_target="tpu_custom_call", output_to_operand_aliasing={{0}: (15, {}), {1}: (16, {})} | custom-call | flops 1073741824 | bytes 4194304 | tf_op jit(solution)/shard_map/pallas_call | solution.py:539
  (120 shorter events, 10.9 us)
Async XLA Ops:
  4.9 26.4 %collective-permute-start.3 = (bf16[128,4096]{1,0:T(8,128)(2,1)}, bf16[128,4096]{1,0:T(8,128)(2,1)S(1)}, u32[]{:S(2)}, u32[]{:S(2)}) collective-permute-start(bf16[128,4096]{1,0:T(8,128)(2,1)} %dynamic-slice_bitcast_fusion), channel_id=1, source_target_pairs={{0,2},{1,3},{2,0},{3,1},{4,6},{5,7},{6,4},{7,5},{8,10},{9,11},{10,... | collective-permute-start | bytes 3145736 | tf_op jit(solution)/shard_map/ppermute | solution.py:67
  7.9 67.7 %collective-permute-start.4 = (bf16[256,4096]{1,0:T(8,128)(2,1)S(1)}, bf16[256,4096]{1,0:T(8,128)(2,1)}, u32[]{:S(2)}, u32[]{:S(2)}) collective-permute-start(bf16[256,4096]{1,0:T(8,128)(2,1)S(1)} %fusion.2.refs_0_), channel_id=1, source_target_pairs={{0,1},{1,0},{2,3},{3,2},{4,5},{5,4},{6,7},{7,6},{8,9},{9,8},{10,11... | collective-permute-start | bytes 6291464 | tf_op jit(solution)/shard_map/ppermute | solution.py:67
  11.3 33.7 %collective-permute-start.10 = (bf16[256,512]{1,0:T(8,128)(2,1)}, bf16[256,512]{1,0:T(8,128)(2,1)}, u32[]{:S(2)}, u32[]{:S(2)}) collective-permute-start(bf16[256,512]{1,0:T(8,128)(2,1)} %dynamic_slice.31), channel_id=1, source_target_pairs={{0,8},{4,12},{8,0},{12,4},{1,9},{5,13},{9,1},{13,5},{2,10},{6,14},... | collective-permute-start | bytes 786440 | tf_op jit(solution)/shard_map/ppermute | solution.py:67
  31.3 43.9 %collective-permute-start.5 = (bf16[128,4096]{1,0:T(8,128)(2,1)S(1)}, bf16[128,4096]{1,0:T(8,128)(2,1)}, u32[]{:S(2)}, u32[]{:S(2)}) collective-permute-start(bf16[128,4096]{1,0:T(8,128)(2,1)S(1)} %collective-permute-done.3.refs_1_), channel_id=1, source_target_pairs={{0,1},{1,0},{2,3},{3,2},{4,5},{5,4},{6,7},{7,6},{8,9},{9,8},{10,11... | collective-permute-start | bytes 3145736 | tf_op jit(solution)/shard_map/ppermute | solution.py:67
  32.8 6.2 %collective-permute-start.1 = (bf16[1,1,32,256]{3,2,1,0:T(8,128)(2,1)S(1)}, bf16[1,1,32,256]{3,2,1,0:T(8,128)(2,1)S(1)}, u32[]{:S(2)}, u32[]{:S(2)}) collective-permute-start(bf16[1,1,32,256]{3,2,1,0:T(8,128)(2,1)S(1)} %bitcast.32), channel_id=1, source_target_pairs={{0,1},{1,0},{2,3},{3,2},{4,5},{5,4},{6,7},{7,6},{8,9},{9,8},{10,11... | collective-permute-start | bytes 49160 | tf_op jit(solution)/shard_map/ppermute | solution.py:67
  37.7 8.8 %collective-permute-start.8 = (bf16[256,512]{1,0:T(8,128)(2,1)}, bf16[256,512]{1,0:T(8,128)(2,1)}, u32[]{:S(2)}, u32[]{:S(2)}) collective-permute-start(bf16[256,512]{1,0:T(8,128)(2,1)} %dynamic_slice.31), channel_id=1, source_target_pairs={{0,4},{4,0},{8,12},{12,8},{1,5},{5,1},{9,13},{13,9},{2,6},{6,2},{1... | collective-permute-start | bytes 786440 | tf_op jit(solution)/shard_map/ppermute | solution.py:67
  39.1 18.0 %collective-permute-start.12 = (bf16[256,512]{1,0:T(8,128)(2,1)}, bf16[256,512]{1,0:T(8,128)(2,1)}, u32[]{:S(2)}, u32[]{:S(2)}) collective-permute-start(bf16[256,512]{1,0:T(8,128)(2,1)} %dynamic_slice.30), channel_id=1, source_target_pairs={{0,12},{4,8},{8,4},{12,0},{1,13},{5,9},{9,5},{13,1},{2,14},{6,10},... | collective-permute-start | bytes 786440 | tf_op jit(solution)/shard_map/ppermute | solution.py:67
  45.0 19.2 %collective-permute-start.16 = (bf16[256,512]{1,0:T(8,128)(2,1)}, bf16[256,512]{1,0:T(8,128)(2,1)}, u32[]{:S(2)}, u32[]{:S(2)}) collective-permute-start(bf16[256,512]{1,0:T(8,128)(2,1)} %dynamic_slice.30), channel_id=1, source_target_pairs={{0,4},{4,0},{8,12},{12,8},{1,5},{5,1},{9,13},{13,9},{2,6},{6,2},{1... | collective-permute-start | bytes 786440 | tf_op jit(solution)/shard_map/ppermute | solution.py:67
  46.5 22.0 %collective-permute-start.6 = (bf16[256,512]{1,0:T(8,128)(2,1)}, bf16[256,512]{1,0:T(8,128)(2,1)}, u32[]{:S(2)}, u32[]{:S(2)}) collective-permute-start(bf16[256,512]{1,0:T(8,128)(2,1)} %dynamic_slice.30), channel_id=1, source_target_pairs={{0,8},{4,12},{8,0},{12,4},{1,9},{5,13},{9,1},{13,5},{2,10},{6,14},... | collective-permute-start | bytes 786440 | tf_op jit(solution)/shard_map/ppermute | solution.py:67
  57.0 12.7 %collective-permute-start.14 = (bf16[256,512]{1,0:T(8,128)(2,1)}, bf16[256,512]{1,0:T(8,128)(2,1)}, u32[]{:S(2)}, u32[]{:S(2)}) collective-permute-start(bf16[256,512]{1,0:T(8,128)(2,1)} %collective-permute-done.12.refs_4_), channel_id=1, source_target_pairs={{0,16},{16,0},{1,17},{17,1},{2,18},{18,2},{3,19},{19,3},{4,20},{20... | collective-permute-start | bytes 786440 | tf_op jit(solution)/shard_map/ppermute | solution.py:67
  64.1 9.5 %collective-permute-start.17 = (bf16[256,512]{1,0:T(8,128)(2,1)}, bf16[256,512]{1,0:T(8,128)(2,1)}, u32[]{:S(2)}, u32[]{:S(2)}) collective-permute-start(bf16[256,512]{1,0:T(8,128)(2,1)} %collective-permute-done.16.refs_6_), channel_id=1, source_target_pairs={{0,16},{16,0},{1,17},{17,1},{2,18},{18,2},{3,19},{19,3},{4,20},{20... | collective-permute-start | bytes 786440 | tf_op jit(solution)/shard_map/ppermute | solution.py:67
  68.6 16.3 %collective-permute-start.13 = (bf16[256,512]{1,0:T(8,128)(2,1)}, bf16[256,512]{1,0:T(8,128)(2,1)}, u32[]{:S(2)}, u32[]{:S(2)}) collective-permute-start(bf16[256,512]{1,0:T(8,128)(2,1)} %collective-permute-done.12.refs_4_), channel_id=1, source_target_pairs={{0,2},{1,3},{2,0},{3,1},{4,6},{5,7},{6,4},{7,5},{8,10},{9,11},{10,... | collective-permute-start | bytes 786440 | tf_op jit(solution)/shard_map/ppermute | solution.py:67
  69.7 13.3 %collective-permute-start.11 = (bf16[256,512]{1,0:T(8,128)(2,1)}, bf16[256,512]{1,0:T(8,128)(2,1)}, u32[]{:S(2)}, u32[]{:S(2)}) collective-permute-start(bf16[256,512]{1,0:T(8,128)(2,1)} %collective-permute-done.10.refs_10_), channel_id=1, source_target_pairs={{0,16},{16,0},{1,17},{17,1},{2,18},{18,2},{3,19},{19,3},{4,20},{20... | collective-permute-start | bytes 786440 | tf_op jit(solution)/shard_map/ppermute | solution.py:67
  73.6 11.2 %collective-permute-start.9 = (bf16[256,512]{1,0:T(8,128)(2,1)}, bf16[256,512]{1,0:T(8,128)(2,1)}, u32[]{:S(2)}, u32[]{:S(2)}) collective-permute-start(bf16[256,512]{1,0:T(8,128)(2,1)} %collective-permute-done.8.refs_9_), channel_id=1, source_target_pairs={{0,16},{16,0},{1,17},{17,1},{2,18},{18,2},{3,19},{19,3},{4,20},{20... | collective-permute-start | bytes 786440 | tf_op jit(solution)/shard_map/ppermute | solution.py:67
  75.1 13.4 %collective-permute-start.7 = (bf16[256,512]{1,0:T(8,128)(2,1)}, bf16[256,512]{1,0:T(8,128)(2,1)}, u32[]{:S(2)}, u32[]{:S(2)}) collective-permute-start(bf16[256,512]{1,0:T(8,128)(2,1)} %collective-permute-done.6.refs_8_), channel_id=1, source_target_pairs={{0,16},{16,0},{1,17},{17,1},{2,18},{18,2},{3,19},{19,3},{4,20},{20... | collective-permute-start | bytes 786440 | tf_op jit(solution)/shard_map/ppermute | solution.py:67
  75.6 12.9 %collective-permute-start.15 = (bf16[256,512]{1,0:T(8,128)(2,1)}, bf16[256,512]{1,0:T(8,128)(2,1)S(1)}, u32[]{:S(2)}, u32[]{:S(2)}) collective-permute-start(bf16[256,512]{1,0:T(8,128)(2,1)} %collective-permute-done.14.refs_5_), channel_id=1, source_target_pairs={{0,2},{1,3},{2,0},{3,1},{4,6},{5,7},{6,4},{7,5},{8,10},{9,11},{10,... | collective-permute-start | bytes 786440 | tf_op jit(solution)/shard_map/ppermute | solution.py:67
  83.0 16.9 %collective-permute-start.2 = (bf16[2,1,32,256]{3,2,1,0:T(8,128)(2,1)S(1)}, bf16[2,1,32,256]{3,2,1,0:T(8,128)(2,1)S(1)}, u32[]{:S(2)}, u32[]{:S(2)}) collective-permute-start(bf16[2,1,32,256]{3,2,1,0:T(8,128)(2,1)S(1)} %pad_maximum_fusion.2), channel_id=1, source_target_pairs={{0,2},{1,3},{2,0},{3,1},{4,6},{5,7},{6,4},{7,5},{8,10},{9,11},{10,... | collective-permute-start | bytes 98312 | tf_op jit(solution)/shard_map/ppermute | solution.py:67
  93.8 6.0 %collective-permute-start.26 = (bf16[128,512]{1,0:T(8,128)(2,1)}, bf16[128,512]{1,0:T(8,128)(2,1)S(1)}, u32[]{:S(2)}, u32[]{:S(2)}) collective-permute-start(bf16[128,512]{1,0:T(8,128)(2,1)} %get-tuple-element.22), channel_id=1, source_target_pairs={{0,4},{4,0},{8,12},{12,8},{1,5},{5,1},{9,13},{13,9},{2,6},{6,2},{1... | collective-permute-start | bytes 393224 | tf_op jit(solution)/shard_map/ppermute | solution.py:67
  94.8 5.6 %collective-permute-start.27 = (bf16[128,512]{1,0:T(8,128)(2,1)}, bf16[128,512]{1,0:T(8,128)(2,1)S(1)}, u32[]{:S(2)}, u32[]{:S(2)}) collective-permute-start(bf16[128,512]{1,0:T(8,128)(2,1)} %get-tuple-element.21.refs_3_), channel_id=1, source_target_pairs={{0,2},{1,3},{2,0},{3,1},{4,6},{5,7},{6,4},{7,5},{8,10},{9,11},{10,... | collective-permute-start | bytes 393224 | tf_op jit(solution)/shard_map/ppermute | solution.py:67
  96.5 3.9 %collective-permute-start.29 = (bf16[128,512]{1,0:T(8,128)(2,1)}, bf16[128,512]{1,0:T(8,128)(2,1)S(1)}, u32[]{:S(2)}, u32[]{:S(2)}) collective-permute-start(bf16[128,512]{1,0:T(8,128)(2,1)} %get-tuple-element.21.refs_3_), channel_id=1, source_target_pairs={{0,1},{1,0},{2,3},{3,2},{4,5},{5,4},{6,7},{7,6},{8,9},{9,8},{10,11... | collective-permute-start | bytes 393224 | tf_op jit(solution)/shard_map/ppermute | solution.py:67
  96.5 12.9 %collective-permute-start.18 = (bf16[128,512]{1,0:T(8,128)(2,1)}, bf16[128,512]{1,0:T(8,128)(2,1)S(1)}, u32[]{:S(2)}, u32[]{:S(2)}) collective-permute-start(bf16[128,512]{1,0:T(8,128)(2,1)} %get-tuple-element.19), channel_id=1, source_target_pairs={{0,8},{4,12},{8,0},{12,4},{1,9},{5,13},{9,1},{13,5},{2,10},{6,14},... | collective-permute-start | bytes 393224 | tf_op jit(solution)/shard_map/ppermute | solution.py:67
  99.9 10.3 %collective-permute-start.19 = (bf16[128,512]{1,0:T(8,128)(2,1)}, bf16[128,512]{1,0:T(8,128)(2,1)S(1)}, u32[]{:S(2)}, u32[]{:S(2)}) collective-permute-start(bf16[128,512]{1,0:T(8,128)(2,1)} %get-tuple-element.20), channel_id=1, source_target_pairs={{0,12},{4,8},{8,4},{12,0},{1,13},{5,9},{9,5},{13,1},{2,14},{6,10},... | collective-permute-start | bytes 393224 | tf_op jit(solution)/shard_map/ppermute | solution.py:67
  99.9 11.5 %collective-permute-start.28 = (bf16[128,512]{1,0:T(8,128)(2,1)S(1)}, bf16[128,512]{1,0:T(8,128)(2,1)S(1)}, u32[]{:S(2)}, u32[]{:S(2)}) collective-permute-start(bf16[128,512]{1,0:T(8,128)(2,1)S(1)} %collective-permute-done.26.refs_4_), channel_id=1, source_target_pairs={{0,2},{1,3},{2,0},{3,1},{4,6},{5,7},{6,4},{7,5},{8,10},{9,11},{10,... | collective-permute-start | bytes 393224 | tf_op jit(solution)/shard_map/ppermute | solution.py:67
  100.3 11.2 %collective-permute-start.30 = (bf16[128,512]{1,0:T(8,128)(2,1)S(1)}, bf16[128,512]{1,0:T(8,128)(2,1)S(1)}, u32[]{:S(2)}, u32[]{:S(2)}) collective-permute-start(bf16[128,512]{1,0:T(8,128)(2,1)S(1)} %collective-permute-done.26.refs_4_), channel_id=1, source_target_pairs={{0,1},{1,0},{2,3},{3,2},{4,5},{5,4},{6,7},{7,6},{8,9},{9,8},{10,11... | collective-permute-start | bytes 393224 | tf_op jit(solution)/shard_map/ppermute | solution.py:67
  100.4 11.8 %collective-permute-start.31 = (bf16[128,512]{1,0:T(8,128)(2,1)S(1)}, bf16[128,512]{1,0:T(8,128)(2,1)S(1)}, u32[]{:S(2)}, u32[]{:S(2)}) collective-permute-start(bf16[128,512]{1,0:T(8,128)(2,1)S(1)} %collective-permute-done.27.refs_5_), channel_id=1, source_target_pairs={{0,1},{1,0},{2,3},{3,2},{4,5},{5,4},{6,7},{7,6},{8,9},{9,8},{10,11... | collective-permute-start | bytes 393224 | tf_op jit(solution)/shard_map/ppermute | solution.py:67
  109.4 6.4 %collective-permute-start.20 = (bf16[128,512]{1,0:T(8,128)(2,1)S(1)}, bf16[128,512]{1,0:T(8,128)(2,1)S(1)}, u32[]{:S(2)}, u32[]{:S(2)}) collective-permute-start(bf16[128,512]{1,0:T(8,128)(2,1)S(1)} %collective-permute-done.18.refs_6_), channel_id=1, source_target_pairs={{0,2},{1,3},{2,0},{3,1},{4,6},{5,7},{6,4},{7,5},{8,10},{9,11},{10,... | collective-permute-start | bytes 393224 | tf_op jit(solution)/shard_map/ppermute | solution.py:67
  110.2 7.5 %collective-permute-start.21 = (bf16[128,512]{1,0:T(8,128)(2,1)S(1)}, bf16[128,512]{1,0:T(8,128)(2,1)S(1)}, u32[]{:S(2)}, u32[]{:S(2)}) collective-permute-start(bf16[128,512]{1,0:T(8,128)(2,1)S(1)} %collective-permute-done.19.refs_7_), channel_id=1, source_target_pairs={{0,2},{1,3},{2,0},{3,1},{4,6},{5,7},{6,4},{7,5},{8,10},{9,11},{10,... | collective-permute-start | bytes 393224 | tf_op jit(solution)/shard_map/ppermute | solution.py:67
  111.5 6.9 %collective-permute-start.32 = (bf16[128,512]{1,0:T(8,128)(2,1)S(1)}, bf16[128,512]{1,0:T(8,128)(2,1)S(1)}, u32[]{:S(2)}, u32[]{:S(2)}) collective-permute-start(bf16[128,512]{1,0:T(8,128)(2,1)S(1)} %collective-permute-done.28.refs_6_), channel_id=1, source_target_pairs={{0,1},{1,0},{2,3},{3,2},{4,5},{5,4},{6,7},{7,6},{8,9},{9,8},{10,11... | collective-permute-start | bytes 393224 | tf_op jit(solution)/shard_map/ppermute | solution.py:67
  111.6 12.1 %collective-permute-start.22 = (bf16[128,512]{1,0:T(8,128)(2,1)S(1)}, bf16[128,512]{1,0:T(8,128)(2,1)S(1)}, u32[]{:S(2)}, u32[]{:S(2)}) collective-permute-start(bf16[128,512]{1,0:T(8,128)(2,1)S(1)} %collective-permute-done.18.refs_6_), channel_id=1, source_target_pairs={{0,1},{1,0},{2,3},{3,2},{4,5},{5,4},{6,7},{7,6},{8,9},{9,8},{10,11... | collective-permute-start | bytes 393224 | tf_op jit(solution)/shard_map/ppermute | solution.py:67
  112.1 11.6 %collective-permute-start.23 = (bf16[128,512]{1,0:T(8,128)(2,1)S(1)}, bf16[128,512]{1,0:T(8,128)(2,1)S(1)}, u32[]{:S(2)}, u32[]{:S(2)}) collective-permute-start(bf16[128,512]{1,0:T(8,128)(2,1)S(1)} %collective-permute-done.19.refs_7_), channel_id=1, source_target_pairs={{0,1},{1,0},{2,3},{3,2},{4,5},{5,4},{6,7},{7,6},{8,9},{9,8},{10,11... | collective-permute-start | bytes 393224 | tf_op jit(solution)/shard_map/ppermute | solution.py:67
  115.8 8.0 %collective-permute-start.24 = (bf16[128,512]{1,0:T(8,128)(2,1)S(1)}, bf16[128,512]{1,0:T(8,128)(2,1)S(1)}, u32[]{:S(2)}, u32[]{:S(2)}) collective-permute-start(bf16[128,512]{1,0:T(8,128)(2,1)S(1)} %collective-permute-done.20.refs_8_), channel_id=1, source_target_pairs={{0,1},{1,0},{2,3},{3,2},{4,5},{5,4},{6,7},{7,6},{8,9},{9,8},{10,11... | collective-permute-start | bytes 393224 | tf_op jit(solution)/shard_map/ppermute | solution.py:67
  117.7 6.1 %collective-permute-start.25 = (bf16[128,512]{1,0:T(8,128)(2,1)S(1)}, bf16[128,512]{1,0:T(8,128)(2,1)S(1)}, u32[]{:S(2)}, u32[]{:S(2)}) collective-permute-start(bf16[128,512]{1,0:T(8,128)(2,1)S(1)} %collective-permute-done.21.refs_9_), channel_id=1, source_target_pairs={{0,1},{1,0},{2,3},{3,2},{4,5},{5,4},{6,7},{7,6},{8,9},{9,8},{10,11... | collective-permute-start | bytes 393224 | tf_op jit(solution)/shard_map/ppermute | solution.py:67
  (34 other events, 1056.2 us)
